TPU v7x, 32 devices: a whole 2x2x4 slice. The times are simulated.
32 devices in a mesh: ep: 4 (over y, x), tp: 8 (over z, core).
Axes of the slice: x: 2, y: 2, z: 4, core: 2. Of those that a mesh axis runs over, the one named last changes fastest.
Arguments:
- tokens: bfloat16 [64, 4096], P('ep'), may hold values from -150 to 150
- query_weight: bfloat16 [4096, 1024], P('tp'), may hold values from -0.09375 to 0.09375
- key_weight: bfloat16 [4096, 1024], P('tp'), may hold values from -0.09375 to 0.09375
- value_weight: bfloat16 [4096, 2048], P(None, 'tp'), may hold values from -0.09375 to 0.09375
- decay_down: bfloat16 [4096, 16], replicated, may hold values from -0.09375 to 0.09375
- decay_up: float32 [16, 1024], replicated, may hold values from -3 to 3
- decay_bias: float32 [1024], replicated, may hold values from -8 to 4
- old_state: float32 [64, 256, 2048], P('ep', None, 'tp'), may hold values from -8 to 8
- out_weight: bfloat16 [2048, 4096], P('tp'), may hold values from -0.1875 to 0.1875
- norm_gain: float32 [4096], replicated, may hold values from 0.2 to 4
- router_weight: bfloat16 [4096, 4], replicated, may hold values from -0.09375 to 0.09375
- routing: int32 [64, 2], P('ep'), may hold values from 0 to 3, all different within a row; in each aligned block of 16 rows (0 to 15, 16 to 31, ...) at most 16 rows name the same one
- glu_weight: bfloat16 [4, 4096, 2048], P('ep', None, 'tp'), may hold values from -0.25 to 0.25
- linear_weight: bfloat16 [4, 4096, 2048], P('ep', None, 'tp'), may hold values from -0.25 to 0.25
- down_weight: bfloat16 [4, 2048, 4096], P('ep', 'tp'), may hold values from -0.01953125 to 0.01953125
- final_gain: float32 [4096], replicated, may hold values from 0.1 to 1.9
Outputs:
- layer_out: bfloat16 [64, 4096], P('ep', 'tp')
- new_state: float32 [64, 256, 2048], P('ep', None, 'tp')
Inputs may be any that keep to these rules, and one draw needn't show every extreme that they name: `routing`: within the rows of one device (aligned blocks of 16 rows) no expert is named by more than 16 rows, and at least one block reaches that bound; each row names 2 different experts.
All inputs are finite; a program needn't handle non-finite values.
Results may differ from a plain program's by a relative error of at most 0.015.
Values may be sent and summed in bfloat16 or wider, within the bound.
A program may use at most 64 MiB of HBM per device.

v0:
```python
import jax
import jax.numpy as jnp
from jax import lax
from jax.sharding import PartitionSpec as P

ALPHA = 2.0**0.25
TAU = 16.0
LIMIT = 7.0
SLOPE = 1.702
EPSILON = 1e-05


def norm_from_totals(inputs, totals, width, gain):
    mean = totals[0][:, None] / width
    variance = totals[1][:, None] / width - mean * mean
    return (inputs - mean) * lax.rsqrt(variance + EPSILON) * gain


def row_totals(inputs):
    return (jnp.sum(inputs, axis=1), jnp.sum(inputs * inputs, axis=1))


def clamped_unit(glu_pre, linear_pre):
    glu = jnp.minimum(glu_pre, LIMIT)
    linear = jnp.clip(linear_pre, -LIMIT, LIMIT)
    return glu * jax.nn.sigmoid(SLOPE * glu) * (linear + 1.0)


def expert_gate(logits, slot_ids, own_expert):
    expert_ids = jnp.arange(logits.shape[1], dtype=jnp.int32)
    picked = jnp.sum(
        jnp.where(slot_ids[:, :, None] == expert_ids[None, None, :], logits[:, None, :], 0.0),
        axis=2,
    )
    own_logit = jnp.sum(jnp.where(expert_ids[None, :] == own_expert, logits, 0.0), axis=1)
    return jnp.exp(own_logit) / jnp.sum(jnp.exp(picked), axis=1)


def per_device(
    tokens,
    query_weight,
    key_weight,
    value_weight,
    decay_down,
    decay_up,
    decay_bias,
    old_state,
    out_weight,
    norm_gain,
    router_weight,
    routing,
    glu_weight,
    linear_weight,
    down_weight,
    final_gain,
):
    tp_count = lax.axis_size("tp")
    tp_rank = lax.axis_index("tp")
    own_expert = lax.axis_index("ep")
    seq_count, width = tokens.shape
    head_dk = old_state.shape[1]
    heads = query_weight.shape[1] // head_dk
    head_start = tp_rank // (tp_count // heads) * head_dk
    top_count = routing.shape[1]
    experts = router_weight.shape[1]
    slot_cap = max(2, (2 * seq_count * top_count + experts - 1) // experts)
    share_width = width // tp_count
    share_start = tp_rank * share_width
    glu_local = glu_weight[0]
    linear_local = linear_weight[0]
    down_local = down_weight[0]
    token_share = lax.dynamic_slice_in_dim(tokens, share_start, share_width, 1)
    query_part = jnp.dot(token_share, query_weight, preferred_element_type=jnp.float32)
    key_part = jnp.dot(token_share, key_weight, preferred_element_type=jnp.float32)
    query_sum, key_sum = lax.psum((query_part, key_part), "tp")
    query_all = query_sum.astype(jnp.bfloat16)
    key_all = key_sum.astype(jnp.bfloat16)
    values = jnp.dot(tokens, value_weight, preferred_element_type=jnp.float32).astype(jnp.bfloat16)
    low_rank = jnp.dot(tokens, decay_down, preferred_element_type=jnp.float32)
    up_cols = lax.dynamic_slice_in_dim(decay_up, head_start, head_dk, 1)
    bias_cols = lax.dynamic_slice_in_dim(decay_bias, head_start, head_dk, 0)
    decay = jnp.exp(
        jax.nn.log_sigmoid(jnp.dot(low_rank, up_cols, precision=lax.Precision.HIGHEST) + bias_cols)
        / TAU
    )
    query = lax.dynamic_slice_in_dim(query_all, head_start, head_dk, 1).astype(jnp.float32)
    keys = lax.dynamic_slice_in_dim(key_all, head_start, head_dk, 1).astype(jnp.float32)
    new_state = (
        decay[:, :, None] * old_state + keys[:, :, None] * values.astype(jnp.float32)[:, None, :]
    )
    mixed = (
        jnp.einsum("si,sic->sc", query, new_state, precision=lax.Precision.HIGHEST)
        * head_dk ** (-0.5)
    ).astype(jnp.bfloat16)
    out_terms = jnp.dot(mixed, out_weight, preferred_element_type=jnp.float32)
    flat_ids = routing.reshape(-1)
    expert_ids = jnp.arange(experts, dtype=jnp.int32)
    chosen = (flat_ids[:, None] == expert_ids[None, :]).astype(jnp.int32)
    before = jnp.cumsum(chosen, axis=0) - chosen
    slot_rank = jnp.sum(before * chosen, axis=1)
    slot_index = flat_ids * slot_cap + slot_rank
    placed = (
        slot_index[:, None] == jnp.arange(experts * slot_cap, dtype=jnp.int32)[None, :]
    ).astype(jnp.int32)
    spread = jnp.sum(placed.reshape(seq_count, top_count, experts * slot_cap), axis=1)
    spread_rows = spread.astype(jnp.bfloat16)
    slot_ids = jnp.einsum("sn,sk->nk", spread, routing).reshape(experts, slot_cap, top_count)
    projected = lax.psum_scatter(out_terms, "tp", scatter_dimension=1, tiled=True)
    hidden_in = ALPHA * token_share.astype(jnp.float32) + projected
    first = lax.psum(row_totals(hidden_in), "tp")
    gain_share = lax.dynamic_slice_in_dim(norm_gain, share_start, share_width, 0)
    normed = norm_from_totals(hidden_in, first, width, gain_share).astype(jnp.bfloat16)
    send_rows = jnp.einsum(
        "sn,sd->nd", spread_rows, normed, preferred_element_type=jnp.float32
    ).astype(jnp.bfloat16)
    send_rows = send_rows.reshape(experts, slot_cap, normed.shape[1])
    rows_in = lax.all_to_all(send_rows, "ep", split_axis=0, concat_axis=0, tiled=True)
    ids_in = lax.all_to_all(slot_ids, "ep", split_axis=0, concat_axis=0, tiled=True)
    sources, slots, row_width = rows_in.shape
    count = sources * slots
    piece = lax.all_gather(rows_in, "tp", axis=2, tiled=True)
    size = piece.shape[2]
    flat = piece.reshape(count, size)
    glu_pre = jnp.dot(flat, glu_local, preferred_element_type=jnp.float32)
    linear_pre = jnp.dot(flat, linear_local, preferred_element_type=jnp.float32)
    logits = jnp.dot(flat, router_weight, preferred_element_type=jnp.float32)
    act = clamped_unit(glu_pre, linear_pre).astype(jnp.bfloat16)
    summed = lax.psum_scatter(
        jnp.dot(act, down_local, preferred_element_type=jnp.float32),
        "tp",
        scatter_dimension=1,
        tiled=True,
    )
    gate = expert_gate(logits, ids_in.reshape(count, top_count), own_expert)
    weighted = (
        (summed * gate[:, None]).astype(jnp.bfloat16).reshape(sources, slots, summed.shape[1])
    )
    returned = lax.all_to_all(weighted, "ep", split_axis=0, concat_axis=0, tiled=True)
    combined = ALPHA * normed.astype(jnp.float32) + jnp.einsum(
        "sn,nd->sd",
        spread_rows,
        returned.reshape(experts * slot_cap, normed.shape[1]),
        preferred_element_type=jnp.float32,
    )
    second = lax.psum(row_totals(combined), "tp")
    final_share = lax.dynamic_slice_in_dim(final_gain, share_start, share_width, 0)
    layer_out = norm_from_totals(combined, second, width, final_share).astype(jnp.bfloat16)
    return (layer_out, new_state)


def solution(mesh):
    return jax.shard_map(
        per_device,
        mesh=mesh,
        in_specs=(
            P("ep", None),
            P("tp", None),
            P("tp", None),
            P(None, "tp"),
            P(),
            P(),
            P(),
            P("ep", None, "tp"),
            P("tp", None),
            P(),
            P(),
            P("ep", None),
            P("ep", None, "tp"),
            P("ep", None, "tp"),
            P("ep", "tp", None),
            P(),
        ),
        out_specs=(P("ep", "tp"), P("ep", None, "tp")),
        check_vma=False,
    )
```

profile of v0, /device:TPU:0, one launch (start us, length us, event | category | flops | bytes accessed | tf_op | source)
XLA Modules:
  0.0 188.1 jit_solution(6148383914185210825)
XLA Ops:
  7.3 1.6 fusion.43
  8.9 1.5 fusion.45
  10.4 31.6 %all-reduce.4 = (bf16[16,1024]{1,0:T(8,128)(2,1)S(1)}, bf16[16,1024]{1,0:T(8,128)(2,1)S(1)}) all-reduce(f32[16,1024]{1,0:T(8,128)S(1)} %fusion.43, f32[16,1024]{1,0:T(8,128)S(1)} %fusion.45), channel_id=1, replica_groups=mesh['ep'=4,'tp'=8] {'tp'}, use_global_device_ids=true, to_apply=%region_1.2 | all-reduce | flops 32768 | bytes 196608 | tf_op jit(solution)/shard_map/psum | solution.py:75
  42.0 0.8 dynamic_slice.24
  42.9 2.0 %fusion.24 = f32[16,256]{1,0:T(8,128)S(1)} fusion(bf16[16,4096]{1,0:T(8,128)(2,1)S(1)} %copy-done.3, bf16[4096,256]{1,0:T(8,128)(2,1)} %param.19), kind=kOutput, calls=%fused_computation.17 | convolution fusion | flops 33562624 | bytes 2244608 | tf_op jit(solution)/shard_map/dot_general | solution.py:78
  44.9 0.9 fusion.37
  45.8 2.9 %multiply_add_fusion = f32[16,256,256]{2,1,0:T(8,128)S(1)} fusion(f32[16,256,256]{2,1,0:T(8,128)} %param.23, f32[16,256]{1,0:T(8,128)S(1)} %fusion.24, f32[16,256]{1,0:T(8,128)S(1)} %fusion.50, f32[16,256]{1,0:T(8,128)S(1)} %fusion.37), kind=kLoop, calls=%fused_computation | loop fusion | flops 3145728 | bytes 8437760 | tf_op jit(solution)/shard_map/add | solution.py:89
  48.7 1.5 fusion.39
  50.2 0.6 copy-done.1
  50.8 1.0 copy-done.2
  51.8 1.1 fusion.47
  53.2 0.8 dynamic_slice.26
  54.5 27.6 %reduce-scatter.3.cloned.1.call-done = f32[16,512]{1,0:T(8,128)} async-done(((f32[16,4096]{1,0:T(8,128)}), f32[16,512]{1,0:T(8,128)}) %reduce-scatter.3.cloned.1.call-update) | async-done | bytes 32784 | tf_op jit(solution)/shard_map/reduce_scatter | solution.py:108
  82.1 0.9 fusion.52
  83.0 13.7 %all-reduce.1 = (f32[16]{0:T(128)S(1)}, f32[16]{0:T(128)S(1)}) all-reduce(f32[16]{0:T(128)S(1)} %get-tuple-element.3, f32[16]{0:T(128)S(1)} %get-tuple-element.2), channel_id=1, replica_groups=mesh['ep'=4,'tp'=8] {'tp'}, use_global_device_ids=true, to_apply=%region_6.7 | all-reduce | flops 32 | bytes 256 | tf_op jit(solution)/shard_map/psum | solution.py:110
  96.7 0.8 multiply_convert_fusion.2
  97.7 8.5 %all_to_all.15 = bf16[4,16,512]{2,1,0:T(8,128)(2,1)S(1)} all-to-all(bf16[4,16,512]{2,1,0:T(8,128)(2,1)S(1)} %bitcast.58), channel_id=1, replica_groups=mesh['ep'=4,'tp'=8] {'ep'}, dimensions={0} | all-to-all | bytes 131072 | tf_op jit(solution)/shard_map/all_to_all | solution.py:117
  106.3 14.9 %all_gather.3 = bf16[4,16,4096]{2,1,0:T(8,128)(2,1)S(1)} all-gather(bf16[4,16,512]{2,1,0:T(8,128)(2,1)S(1)} %all_to_all.15), channel_id=1, replica_groups=mesh['ep'=4,'tp'=8] {'tp'}, dimensions={2}, use_global_device_ids=true | all-gather | bytes 589824 | tf_op jit(solution)/shard_map/all_gather | solution.py:121
  121.2 2.0 %fusion.6 = f32[64,256]{1,0:T(8,128)S(1)} fusion(bf16[64,4096]{1,0:T(8,128)(2,1)S(1)} %bitcast.55, bf16[1,4096,256]{2,1,0:T(8,128)(2,1)} %param.28), kind=kOutput, calls=%fused_computation.8 | convolution fusion | flops 134234112 | bytes 2686976 | tf_op jit(solution)/shard_map/dot_general | solution.py:124
  123.3 4.0 %fusion = f32[64,4096]{1,0:T(8,128)} fusion(bf16[1,256,4096]{2,1,0:T(8,128)(2,1)S(1)} %copy-done, bf16[64,4096]{1,0:T(8,128)(2,1)S(1)} %bitcast.56, bf16[1,4096,256]{2,1,0:T(8,128)(2,1)} %param.29, f32[64,256]{1,0:T(8,128)S(1)} %fusion.6), kind=kOutput, calls=%fused_computation.1 | convolution fusion | flops 268582912 | bytes 5832704 | tf_op jit(solution)/shard_map/dot_general | solution.py:129
  127.4 1.1 fusion.55
  128.5 3.2 %all-to-all-start.1 = ((s32[4,16,2]{1,2,0:T(2,128)}), s32[4,16,2]{1,2,0:T(2,128)S(1)}, u32[]{:S(2)}, u32[]{:S(2)}) async-start(s32[4,16,2]{1,2,0:T(2,128)} %fusion.55), calls=%async_computation.3 | async-start | bytes 8192 | tf_op jit(solution)/shard_map/all_to_all | solution.py:118
  131.7 4.6 %all-to-all-done.1 = s32[4,16,2]{1,2,0:T(2,128)S(1)} async-done(((s32[4,16,2]{1,2,0:T(2,128)}), s32[4,16,2]{1,2,0:T(2,128)S(1)}, u32[]{:S(2)}, u32[]{:S(2)}) %all-to-all-start.1) | async-done | bytes 544 | tf_op jit(solution)/shard_map/all_to_all | solution.py:118
  136.5 0.3 select_reduce_fusion.2
  136.8 19.8 %reduce-scatter.5.cloned.1.call-done = f32[64,512]{1,0:T(8,128)} async-done(((f32[64,4096]{1,0:T(8,128)}), f32[64,512]{1,0:T(8,128)}) %reduce-scatter.5.cloned.1.call-update) | async-done | bytes 131088 | tf_op jit(solution)/shard_map/reduce_scatter | solution.py:128
  156.6 1.6 multiply_convert_fusion
  158.2 3.7 %all-to-all-start.2 = ((bf16[4,16,512]{2,1,0:T(8,128)(2,1)}), bf16[4,16,512]{2,1,0:T(8,128)(2,1)S(1)}, u32[]{:S(2)}, u32[]{:S(2)}) async-start(bf16[4,16,512]{2,1,0:T(8,128)(2,1)} %bitcast.10), calls=%async_computation.4 | async-start | bytes 131072 | tf_op jit(solution)/shard_map/all_to_all | solution.py:138
  161.9 0.8 dynamic_slice.27
  162.7 4.1 %all-to-all-done.2 = bf16[4,16,512]{2,1,0:T(8,128)(2,1)S(1)} async-done(((bf16[4,16,512]{2,1,0:T(8,128)(2,1)}), bf16[4,16,512]{2,1,0:T(8,128)(2,1)S(1)}, u32[]{:S(2)}, u32[]{:S(2)}) %all-to-all-start.2) | async-done | bytes 65568 | tf_op jit(solution)/shard_map/all_to_all | solution.py:138
  166.8 0.2 fusion.65
  167.0 13.6 %all-reduce = (f32[16]{0:T(128)S(1)}, f32[16]{0:T(128)S(1)}) all-reduce(f32[16]{0:T(128)S(1)} %get-tuple-element.5, f32[16]{0:T(128)S(1)} %get-tuple-element.4), channel_id=1, replica_groups=mesh['ep'=4,'tp'=8] {'tp'}, use_global_device_ids=true, to_apply=%region_17.18 | all-reduce | flops 32 | bytes 256 | tf_op jit(solution)/shard_map/psum | solution.py:145
  180.6 0.7 multiply_convert_fusion.1
  (38 shorter events, 1.5 us)
Async XLA Ops:
  7.2 116.1 %copy-start = (bf16[1,256,4096]{2,1,0:T(8,128)(2,1)S(1)}, bf16[1,256,4096]{2,1,0:T(8,128)(2,1)}, u32[]{:S(2)}) copy-start(bf16[1,256,4096]{2,1,0:T(8,128)(2,1)} %param.30) | copy-start | bytes 6291460
  7.2 35.6 %copy-start.3 = (bf16[16,4096]{1,0:T(8,128)(2,1)S(1)}, bf16[16,4096]{1,0:T(8,128)(2,1)}, u32[]{:S(2)}) copy-start(bf16[16,4096]{1,0:T(8,128)(2,1)} %param.16) | copy-start | bytes 393220
  7.2 35.6 %copy-start.4 = (bf16[4096,16]{0,1:T(8,128)(2,1)S(1)}, bf16[4096,16]{0,1:T(8,128)(2,1)}, u32[]{:S(2)}) copy-start(bf16[4096,16]{0,1:T(8,128)(2,1)} %param.20) | copy-start | bytes 393220
  7.2 74.9 %reduce-scatter.3.cloned.1.call-start = ((), (), s32[]{:S(2)}) async-start(), calls=%async_computation.5 | async-start | bytes 294912 | tf_op jit(solution)/shard_map/reduce_scatter | solution.py:108
  48.7 2.1 %copy-start.1 = (f32[16,256,256]{2,1,0:T(8,128)}, f32[16,256,256]{2,1,0:T(8,128)S(1)}, u32[]{:S(2)}) copy-start(f32[16,256,256]{2,1,0:T(8,128)S(1)} %multiply_add_fusion) | copy-start | bytes 12582916
  48.7 3.1 %copy-start.2 = (bf16[256,4096]{1,0:T(8,128)(2,1)S(1)}, bf16[256,4096]{1,0:T(8,128)(2,1)}, u32[]{:S(2)}) copy-start(bf16[256,4096]{1,0:T(8,128)(2,1)} %param.24) | copy-start | bytes 6291460
  51.8 1.2 copy-start.5
  52.9 103.7 %reduce-scatter.5.cloned.1.call-start = ((), (), s32[]{:S(2)}) async-start(), calls=%async_computation.6 | async-start | bytes 1179648 | tf_op jit(solution)/shard_map/reduce_scatter | solution.py:128
  123.3 13.2 %copy-start.6 = (bf16[4096,4]{0,1:T(4,128)(2,1)S(1)}, bf16[4096,4]{0,1:T(4,128)(2,1)}, u32[]{:S(2)}) copy-start(bf16[4096,4]{0,1:T(4,128)(2,1)} %param.26) | copy-start | bytes 98308
  128.5 7.9 %all-to-all-start.1 = ((s32[4,16,2]{1,2,0:T(2,128)}), s32[4,16,2]{1,2,0:T(2,128)S(1)}, u32[]{:S(2)}, u32[]{:S(2)}) async-start(s32[4,16,2]{1,2,0:T(2,128)} %fusion.55), calls=%async_computation.3 | async-start | bytes 8192 | tf_op jit(solution)/shard_map/all_to_all | solution.py:118
  158.2 8.6 %all-to-all-start.2 = ((bf16[4,16,512]{2,1,0:T(8,128)(2,1)}), bf16[4,16,512]{2,1,0:T(8,128)(2,1)S(1)}, u32[]{:S(2)}, u32[]{:S(2)}) async-start(bf16[4,16,512]{2,1,0:T(8,128)(2,1)} %bitcast.10), calls=%async_computation.4 | async-start | bytes 131072 | tf_op jit(solution)/shard_map/all_to_all | solution.py:138
Sparse Core Ops, SparseCore 0:
  53.0 28.9 reduce-scatter.2
  127.4 29.1 reduce-scatter.4
where the time goes:
time: 189 us; the launch traced here: 188 us
  blocking collectives  82.4 us (44%)
  waiting for transfers between devices  56.2 us (30%)
  matrix products  16.6 us (9%)
  between operations  14.2 us (8%)
  other arithmetic  7.34 us (4%)
  starting transfers between devices  7.03 us (4%)
  local copies, waits for them, and re-layouts  4.41 us (2%)
    psum x1, blocking collectives, per_device(): query_sum, key_sum = lax.psum((query_part, key_part), 'tp')  31.6 us
    reduce_scatter x1, waiting for transfers between devices, per_device(): lax.psum_scatter(out_terms, 'tp', scatter_dimension=1, tiled=True)  27.6 us
    reduce_scatter x1, waiting for transfers between devices, per_device(): lax.psum_scatter(jnp.dot(act, down_local, preferred_element_type=jnp.floa...  19.8 us
    all_gather x1, blocking collectives, per_device(): piece = lax.all_gather(rows_in, 'tp', axis=2, tiled=True)  14.9 us
    psum x1, blocking collectives, per_device(): first = lax.psum(row_totals(hidden_in), 'tp')  13.7 us
    psum x1, blocking collectives, per_device(): second = lax.psum(row_totals(combined), 'tp')  13.6 us
    all_to_all x1, blocking collectives, per_device(): lax.all_to_all(send_rows, 'ep', split_axis=0, concat_axis=0, tiled=True)  8.53 us
    all_to_all x1, waiting for transfers between devices, per_device(): lax.all_to_all(slot_ids, 'ep', split_axis=0, concat_axis=0, tiled=True)  4.63 us
  transfers between devices with their start and end apart: 4, of which 4 were waited for; matrix products, arithmetic and copies ran while one was open for 2% of the time, Pallas kernels for 0%

commit v1 on v0

--- a/solution.py
+++ b/solution.py
@@ -118,7 +118,27 @@
     ids_in = lax.all_to_all(slot_ids, "ep", split_axis=0, concat_axis=0, tiled=True)
     sources, slots, row_width = rows_in.shape
     count = sources * slots
-    piece = lax.all_gather(rows_in, "tp", axis=2, tiled=True)
+    earlier = lax.psum(1, "tp")
+    u_next = lax.axis_index("tp")
+    block_out, k_now, frame_out = (earlier, u_next, rows_in.shape[2])
+    ledger = tuple(
+        (pp * block_out if hop_no == 2 else pp for hop_no, pp in enumerate(rows_in.shape))
+    )
+    block_now = jnp.zeros(ledger, rows_in.dtype)
+    mat_out = b_now = rows_in
+    piece = lax.dynamic_update_slice_in_dim(block_now, rows_in, k_now * frame_out, axis=2)
+    for j in range(1, block_out // 2 + 1):
+        g_now = tuple(((hop_no, (hop_no + 1) % block_out) for hop_no in range(block_out)))
+        mat_out = lax.ppermute(mat_out, "tp", g_now)
+        piece = lax.dynamic_update_slice_in_dim(
+            piece, mat_out, (k_now - j) % block_out * frame_out, axis=2
+        )
+        if 2 * j < block_out:
+            kept_arr = tuple(((hop_no, (hop_no - 1) % block_out) for hop_no in range(block_out)))
+            b_now = lax.ppermute(b_now, "tp", kept_arr)
+            piece = lax.dynamic_update_slice_in_dim(
+                piece, b_now, (k_now + j) % block_out * frame_out, axis=2
+            )
     size = piece.shape[2]
     flat = piece.reshape(count, size)
     glu_pre = jnp.dot(flat, glu_local, preferred_element_type=jnp.float32)

time: 189 us -> 197 us (1.042)
  blocking collectives: 82.4 us -> 58.9 us
  waiting for transfers between devices: 56.2 us -> 72.3 us
  starting transfers between devices: 7.03 us -> 21.6 us
    all_gather x1 -> x0, blocking collectives: 14.9 us -> none  [per_device(): piece = lax.all_gather(rows_in, 'tp', axis=2, tiled=True)]
    ppermute x0 -> x7, waiting for transfers between devices: none -> 11.3 us  [the longest x4 11.3 us: per_device(): mat_out = lax.ppermute(mat_out, 'tp', g_now)]
    ppermute x0 -> x7, starting transfers between devices: none -> 10.6 us  [the longest x3 10.6 us: per_device(): b_now = lax.ppermute(b_now, 'tp', kept_arr)]
    all_to_all x1 -> x0, blocking collectives: 8.53 us -> none  [per_device(): lax.all_to_all(send_rows, 'ep', split_axis=0, concat_axis=0, tiled=True)]
    all_to_all x0 -> x1, waiting for transfers between devices: none -> 4.84 us  [per_device(): lax.all_to_all(send_rows, 'ep', split_axis=0, concat_axis=0, tiled=True)]
    all_to_all x0 -> x1, starting transfers between devices: none -> 3.88 us  [per_device(): lax.all_to_all(send_rows, 'ep', split_axis=0, concat_axis=0, tiled=True)]
  transfers between devices with their start and end apart: 4 -> 12, of which waited for: 4 -> 9; matrix products, arithmetic and copies ran while one was open for 2% -> 2% of each run, Pallas kernels for 0% -> 0%
where the time goes in v1:
time: 197 us; the launch traced here: 196 us
  waiting for transfers between devices  72.3 us (37%)
  blocking collectives  58.9 us (30%)
  starting transfers between devices  21.6 us (11%)
  matrix products  17.2 us (9%)
  between operations  14.3 us (7%)
  other arithmetic  7.34 us (4%)
  local copies, waits for them, and re-layouts  4.53 us (2%)
    psum x1, blocking collectives, per_device(): query_sum, key_sum = lax.psum((query_part, key_part), 'tp')  31.6 us
    reduce_scatter x1, waiting for transfers between devices, per_device(): lax.psum_scatter(out_terms, 'tp', scatter_dimension=1, tiled=True)  27.7 us
    reduce_scatter x1, waiting for transfers between devices, per_device(): lax.psum_scatter(jnp.dot(act, down_local, preferred_element_type=jnp.floa...  19.8 us
    psum x1, blocking collectives, per_device(): first = lax.psum(row_totals(hidden_in), 'tp')  13.7 us
    psum x1, blocking collectives, per_device(): second = lax.psum(row_totals(combined), 'tp')  13.6 us
    ppermute x4, waiting for transfers between devices, per_device(): mat_out = lax.ppermute(mat_out, 'tp', g_now)  11.3 us
    ppermute x3, starting transfers between devices, per_device(): b_now = lax.ppermute(b_now, 'tp', kept_arr)  10.6 us
    all_to_all x1, waiting for transfers between devices, per_device(): lax.all_to_all(send_rows, 'ep', split_axis=0, concat_axis=0, tiled=True)  4.84 us
  transfers between devices with their start and end apart: 12, of which 9 were waited for; matrix products, arithmetic and copies ran while one was open for 2% of the time, Pallas kernels for 0%

profile of v1, /device:TPU:0, one launch (start us, length us, event | category | flops | bytes accessed | tf_op | source)
XLA Modules:
  0.0 196.2 jit_solution(13733827087048339835)
XLA Ops:
  7.3 1.6 fusion.33
  8.9 1.5 fusion.35
  10.4 31.6 %all-reduce.4 = (bf16[16,1024]{1,0:T(8,128)(2,1)S(1)}, bf16[16,1024]{1,0:T(8,128)(2,1)S(1)}) all-reduce(f32[16,1024]{1,0:T(8,128)S(1)} %fusion.33, f32[16,1024]{1,0:T(8,128)S(1)} %fusion.35), channel_id=1, replica_groups=mesh['ep'=4,'tp'=8] {'tp'}, use_global_device_ids=true, to_apply=%region_1.2 | all-reduce | flops 32768 | bytes 196608 | tf_op jit(solution)/shard_map/psum | solution.py:75
  42.9 2.0 %fusion.16 = f32[16,256]{1,0:T(8,128)S(1)} fusion(bf16[16,4096]{1,0:T(8,128)(2,1)S(1)} %copy-done.3, bf16[4096,256]{1,0:T(8,128)(2,1)} %param.19), kind=kOutput, calls=%fused_computation.15 | convolution fusion | flops 33562624 | bytes 2244608 | tf_op jit(solution)/shard_map/dot_general | solution.py:78
  44.9 0.9 fusion.27
  45.8 2.9 %multiply_add_fusion = f32[16,256,256]{2,1,0:T(8,128)S(1)} fusion(f32[16,256,256]{2,1,0:T(8,128)} %param.23, f32[16,256]{1,0:T(8,128)S(1)} %fusion.16, f32[16,256]{1,0:T(8,128)S(1)} %fusion.40, f32[16,256]{1,0:T(8,128)S(1)} %fusion.27), kind=kLoop, calls=%fused_computation | loop fusion | flops 3145728 | bytes 8437760 | tf_op jit(solution)/shard_map/add | solution.py:89
  48.7 1.5 fusion.29
  50.8 1.0 copy-done.2
  51.8 1.1 fusion.37
  54.4 27.7 %reduce-scatter.3.cloned.1.call-done = f32[16,512]{1,0:T(8,128)} async-done(((f32[16,4096]{1,0:T(8,128)}), f32[16,512]{1,0:T(8,128)}) %reduce-scatter.3.cloned.1.call-update) | async-done | bytes 32784 | tf_op jit(solution)/shard_map/reduce_scatter | solution.py:108
  82.1 0.9 fusion.42
  83.0 13.7 %all-reduce.1 = (f32[16]{0:T(128)S(1)}, f32[16]{0:T(128)S(1)}) all-reduce(f32[16]{0:T(128)S(1)} %get-tuple-element.3, f32[16]{0:T(128)S(1)} %get-tuple-element.2), channel_id=1, replica_groups=mesh['ep'=4,'tp'=8] {'tp'}, use_global_device_ids=true, to_apply=%region_6.7 | all-reduce | flops 32 | bytes 256 | tf_op jit(solution)/shard_map/psum | solution.py:110
  96.7 0.8 multiply_convert_fusion.4
  98.4 3.9 %all-to-all-start = ((bf16[4,16,512]{2,1,0:T(8,128)(2,1)}), bf16[4,16,512]{2,1,0:T(8,128)(2,1)S(1)}, u32[]{:S(2)}, u32[]{:S(2)}) async-start(bf16[4,16,512]{2,1,0:T(8,128)(2,1)} %bitcast.2), calls=%async_computation.1 | async-start | bytes 131072 | tf_op jit(solution)/shard_map/all_to_all | solution.py:117
  102.3 4.8 %all-to-all-done = bf16[4,16,512]{2,1,0:T(8,128)(2,1)S(1)} async-done(((bf16[4,16,512]{2,1,0:T(8,128)(2,1)}), bf16[4,16,512]{2,1,0:T(8,128)(2,1)S(1)}, u32[]{:S(2)}, u32[]{:S(2)}) %all-to-all-start) | async-done | bytes 65568 | tf_op jit(solution)/shard_map/all_to_all | solution.py:117
  107.1 3.5 %collective-permute-start.1 = (bf16[4,16,512]{2,1,0:T(8,128)(2,1)S(1)}, bf16[4,16,512]{2,1,0:T(8,128)(2,1)S(1)}, u32[]{:S(2)}, u32[]{:S(2)}) collective-permute-start(bf16[4,16,512]{2,1,0:T(8,128)(2,1)S(1)} %all-to-all-done), channel_id=1, source_target_pairs={{0,7},{1,0},{2,1},{3,2},{4,3},{5,4},{6,5},{7,6},{8,15},{9,8},{10,9... | collective-permute-start | bytes 196616 | tf_op jit(solution)/shard_map/ppermute | solution.py:138
  110.7 1.9 collective-permute-done
  112.6 3.5 %collective-permute-start.3 = (bf16[4,16,512]{2,1,0:T(8,128)(2,1)S(1)}, bf16[4,16,512]{2,1,0:T(8,128)(2,1)S(1)}, u32[]{:S(2)}, u32[]{:S(2)}) collective-permute-start(bf16[4,16,512]{2,1,0:T(8,128)(2,1)S(1)} %collective-permute-done.1), channel_id=1, source_target_pairs={{0,7},{1,0},{2,1},{3,2},{4,3},{5,4},{6,5},{7,6},{8,15},{9,8},{10,9... | collective-permute-start | bytes 196616 | tf_op jit(solution)/shard_map/ppermute | solution.py:138
  116.2 2.0 %collective-permute-done.2 = bf16[4,16,512]{2,1,0:T(8,128)(2,1)S(1)} collective-permute-done((bf16[4,16,512]{2,1,0:T(8,128)(2,1)S(1)}, bf16[4,16,512]{2,1,0:T(8,128)(2,1)S(1)}, u32[]{:S(2)}, u32[]{:S(2)}) %collective-permute-start.2) | collective-permute-done | bytes 65568 | tf_op jit(solution)/shard_map/ppermute | solution.py:132
  118.2 3.5 %collective-permute-start.5 = (bf16[4,16,512]{2,1,0:T(8,128)(2,1)S(1)}, bf16[4,16,512]{2,1,0:T(8,128)(2,1)S(1)}, u32[]{:S(2)}, u32[]{:S(2)}) collective-permute-start(bf16[4,16,512]{2,1,0:T(8,128)(2,1)S(1)} %collective-permute-done.3), channel_id=1, source_target_pairs={{0,7},{1,0},{2,1},{3,2},{4,3},{5,4},{6,5},{7,6},{8,15},{9,8},{10,9... | collective-permute-start | bytes 196616 | tf_op jit(solution)/shard_map/ppermute | solution.py:138
  121.8 1.9 collective-permute-done.4
  123.8 5.4 %collective-permute-done.6 = bf16[4,16,512]{2,1,0:T(8,128)(2,1)S(1)} collective-permute-done((bf16[4,16,512]{2,1,0:T(8,128)(2,1)S(1)}, bf16[4,16,512]{2,1,0:T(8,128)(2,1)S(1)}, u32[]{:S(2)}, u32[]{:S(2)}) %collective-permute-start.6) | collective-permute-done | bytes 65568 | tf_op jit(solution)/shard_map/ppermute | solution.py:132
  129.2 2.1 %fusion.6 = f32[64,256]{1,0:T(8,128)S(1)} fusion(bf16[64,4096]{1,0:T(8,128)(2,1)S(1)} %bitcast.53, bf16[1,4096,256]{2,1,0:T(8,128)(2,1)} %param.28), kind=kOutput, calls=%fused_computation.8 | convolution fusion | flops 134234112 | bytes 2686976 | tf_op jit(solution)/shard_map/dot_general | solution.py:144
  131.3 4.0 %fusion = f32[64,4096]{1,0:T(8,128)} fusion(bf16[1,256,4096]{2,1,0:T(8,128)(2,1)S(1)} %copy-done, f32[64,256]{1,0:T(8,128)S(1)} %fusion.6, bf16[64,4096]{1,0:T(8,128)(2,1)S(1)} %bitcast.54, bf16[1,4096,256]{2,1,0:T(8,128)(2,1)} %param.29), kind=kOutput, calls=%fused_computation.1 | convolution fusion | flops 268582912 | bytes 5832704 | tf_op jit(solution)/shard_map/dot_general | solution.py:149
  135.4 1.1 fusion.48
  136.5 3.2 %all-to-all-start.1 = ((s32[4,16,2]{1,2,0:T(2,128)}), s32[4,16,2]{1,2,0:T(2,128)S(1)}, u32[]{:S(2)}, u32[]{:S(2)}) async-start(s32[4,16,2]{1,2,0:T(2,128)} %fusion.48), calls=%async_computation.3 | async-start | bytes 8192 | tf_op jit(solution)/shard_map/all_to_all | solution.py:118
  139.8 4.6 %all-to-all-done.1 = s32[4,16,2]{1,2,0:T(2,128)S(1)} async-done(((s32[4,16,2]{1,2,0:T(2,128)}), s32[4,16,2]{1,2,0:T(2,128)S(1)}, u32[]{:S(2)}, u32[]{:S(2)}) %all-to-all-start.1) | async-done | bytes 544 | tf_op jit(solution)/shard_map/all_to_all | solution.py:118
  144.8 19.8 %reduce-scatter.5.cloned.1.call-done = f32[64,512]{1,0:T(8,128)} async-done(((f32[64,4096]{1,0:T(8,128)}), f32[64,512]{1,0:T(8,128)}) %reduce-scatter.5.cloned.1.call-update) | async-done | bytes 131088 | tf_op jit(solution)/shard_map/reduce_scatter | solution.py:148
  164.6 1.6 multiply_convert_fusion
  166.2 3.8 %all-to-all-start.2 = ((bf16[4,16,512]{2,1,0:T(8,128)(2,1)}), bf16[4,16,512]{2,1,0:T(8,128)(2,1)S(1)}, u32[]{:S(2)}, u32[]{:S(2)}) async-start(bf16[4,16,512]{2,1,0:T(8,128)(2,1)} %bitcast.10), calls=%async_computation.4 | async-start | bytes 131072 | tf_op jit(solution)/shard_map/all_to_all | solution.py:158
  170.7 4.1 %all-to-all-done.2 = bf16[4,16,512]{2,1,0:T(8,128)(2,1)S(1)} async-done(((bf16[4,16,512]{2,1,0:T(8,128)(2,1)}), bf16[4,16,512]{2,1,0:T(8,128)(2,1)S(1)}, u32[]{:S(2)}, u32[]{:S(2)}) %all-to-all-start.2) | async-done | bytes 65568 | tf_op jit(solution)/shard_map/all_to_all | solution.py:158
  175.0 13.6 %all-reduce = (f32[16]{0:T(128)S(1)}, f32[16]{0:T(128)S(1)}) all-reduce(f32[16]{0:T(128)S(1)} %get-tuple-element.5, f32[16]{0:T(128)S(1)} %get-tuple-element.4), channel_id=1, replica_groups=mesh['ep'=4,'tp'=8] {'tp'}, use_global_device_ids=true, to_apply=%region_17.18 | all-reduce | flops 32 | bytes 256 | tf_op jit(solution)/shard_map/psum | solution.py:165
  (61 shorter events, 6.3 us)
Async XLA Ops:
  7.2 124.1 %copy-start = (bf16[1,256,4096]{2,1,0:T(8,128)(2,1)S(1)}, bf16[1,256,4096]{2,1,0:T(8,128)(2,1)}, u32[]{:S(2)}) copy-start(bf16[1,256,4096]{2,1,0:T(8,128)(2,1)} %param.30) | copy-start | bytes 6291460
  7.2 35.6 %copy-start.3 = (bf16[16,4096]{1,0:T(8,128)(2,1)S(1)}, bf16[16,4096]{1,0:T(8,128)(2,1)}, u32[]{:S(2)}) copy-start(bf16[16,4096]{1,0:T(8,128)(2,1)} %param.16) | copy-start | bytes 393220
  7.2 35.6 %copy-start.4 = (bf16[4096,16]{0,1:T(8,128)(2,1)S(1)}, bf16[4096,16]{0,1:T(8,128)(2,1)}, u32[]{:S(2)}) copy-start(bf16[4096,16]{0,1:T(8,128)(2,1)} %param.20) | copy-start | bytes 393220
  7.2 74.9 %reduce-scatter.3.cloned.1.call-start = ((), (), s32[]{:S(2)}) async-start(), calls=%async_computation.5 | async-start | bytes 294912 | tf_op jit(solution)/shard_map/reduce_scatter | solution.py:108
  48.7 2.1 %copy-start.1 = (f32[16,256,256]{2,1,0:T(8,128)}, f32[16,256,256]{2,1,0:T(8,128)S(1)}, u32[]{:S(2)}) copy-start(f32[16,256,256]{2,1,0:T(8,128)S(1)} %multiply_add_fusion) | copy-start | bytes 12582916
  48.7 3.1 %copy-start.2 = (bf16[256,4096]{1,0:T(8,128)(2,1)S(1)}, bf16[256,4096]{1,0:T(8,128)(2,1)}, u32[]{:S(2)}) copy-start(bf16[256,4096]{1,0:T(8,128)(2,1)} %param.24) | copy-start | bytes 6291460
  51.8 1.1 copy-start.5
  98.4 8.7 %all-to-all-start = ((bf16[4,16,512]{2,1,0:T(8,128)(2,1)}), bf16[4,16,512]{2,1,0:T(8,128)(2,1)S(1)}, u32[]{:S(2)}, u32[]{:S(2)}) async-start(bf16[4,16,512]{2,1,0:T(8,128)(2,1)} %bitcast.2), calls=%async_computation.1 | async-start | bytes 131072 | tf_op jit(solution)/shard_map/all_to_all | solution.py:117
  102.2 62.3 %reduce-scatter.5.cloned.1.call-start = ((), (), s32[]{:S(2)}) async-start(), calls=%async_computation.6 | async-start | bytes 1179648 | tf_op jit(solution)/shard_map/reduce_scatter | solution.py:148
  107.1 5.5 %collective-permute-start = (bf16[4,16,512]{2,1,0:T(8,128)(2,1)S(1)}, bf16[4,16,512]{2,1,0:T(8,128)(2,1)S(1)}, u32[]{:S(2)}, u32[]{:S(2)}) collective-permute-start(bf16[4,16,512]{2,1,0:T(8,128)(2,1)S(1)} %all-to-all-done), channel_id=1, source_target_pairs={{0,1},{1,2},{2,3},{3,4},{4,5},{5,6},{6,7},{7,0},{8,9},{9,10},{10,1... | collective-permute-start | bytes 196616 | tf_op jit(solution)/shard_map/ppermute | solution.py:132
  107.1 5.5 %collective-permute-start.1 = (bf16[4,16,512]{2,1,0:T(8,128)(2,1)S(1)}, bf16[4,16,512]{2,1,0:T(8,128)(2,1)S(1)}, u32[]{:S(2)}, u32[]{:S(2)}) collective-permute-start(bf16[4,16,512]{2,1,0:T(8,128)(2,1)S(1)} %all-to-all-done), channel_id=1, source_target_pairs={{0,7},{1,0},{2,1},{3,2},{4,3},{5,4},{6,5},{7,6},{8,15},{9,8},{10,9... | collective-permute-start | bytes 196616 | tf_op jit(solution)/shard_map/ppermute | solution.py:138
  112.6 5.6 %collective-permute-start.2 = (bf16[4,16,512]{2,1,0:T(8,128)(2,1)S(1)}, bf16[4,16,512]{2,1,0:T(8,128)(2,1)S(1)}, u32[]{:S(2)}, u32[]{:S(2)}) collective-permute-start(bf16[4,16,512]{2,1,0:T(8,128)(2,1)S(1)} %collective-permute-done), channel_id=1, source_target_pairs={{0,1},{1,2},{2,3},{3,4},{4,5},{5,6},{6,7},{7,0},{8,9},{9,10},{10,1... | collective-permute-start | bytes 196616 | tf_op jit(solution)/shard_map/ppermute | solution.py:132
  112.6 5.6 %collective-permute-start.3 = (bf16[4,16,512]{2,1,0:T(8,128)(2,1)S(1)}, bf16[4,16,512]{2,1,0:T(8,128)(2,1)S(1)}, u32[]{:S(2)}, u32[]{:S(2)}) collective-permute-start(bf16[4,16,512]{2,1,0:T(8,128)(2,1)S(1)} %collective-permute-done.1), channel_id=1, source_target_pairs={{0,7},{1,0},{2,1},{3,2},{4,3},{5,4},{6,5},{7,6},{8,15},{9,8},{10,9... | collective-permute-start | bytes 196616 | tf_op jit(solution)/shard_map/ppermute | solution.py:138
  118.2 5.5 %collective-permute-start.4 = (bf16[4,16,512]{2,1,0:T(8,128)(2,1)S(1)}, bf16[4,16,512]{2,1,0:T(8,128)(2,1)S(1)}, u32[]{:S(2)}, u32[]{:S(2)}) collective-permute-start(bf16[4,16,512]{2,1,0:T(8,128)(2,1)S(1)} %collective-permute-done.2), channel_id=1, source_target_pairs={{0,1},{1,2},{2,3},{3,4},{4,5},{5,6},{6,7},{7,0},{8,9},{9,10},{10,1... | collective-permute-start | bytes 196616 | tf_op jit(solution)/shard_map/ppermute | solution.py:132
  118.2 5.5 %collective-permute-start.5 = (bf16[4,16,512]{2,1,0:T(8,128)(2,1)S(1)}, bf16[4,16,512]{2,1,0:T(8,128)(2,1)S(1)}, u32[]{:S(2)}, u32[]{:S(2)}) collective-permute-start(bf16[4,16,512]{2,1,0:T(8,128)(2,1)S(1)} %collective-permute-done.3), channel_id=1, source_target_pairs={{0,7},{1,0},{2,1},{3,2},{4,3},{5,4},{6,5},{7,6},{8,15},{9,8},{10,9... | collective-permute-start | bytes 196616 | tf_op jit(solution)/shard_map/ppermute | solution.py:138
  123.7 5.5 %collective-permute-start.6 = (bf16[4,16,512]{2,1,0:T(8,128)(2,1)S(1)}, bf16[4,16,512]{2,1,0:T(8,128)(2,1)S(1)}, u32[]{:S(2)}, u32[]{:S(2)}) collective-permute-start(bf16[4,16,512]{2,1,0:T(8,128)(2,1)S(1)} %collective-permute-done.4), channel_id=1, source_target_pairs={{0,1},{1,2},{2,3},{3,4},{4,5},{5,6},{6,7},{7,0},{8,9},{9,10},{10,1... | collective-permute-start | bytes 196616 | tf_op jit(solution)/shard_map/ppermute | solution.py:132
  131.3 13.2 %copy-start.6 = (bf16[4096,4]{0,1:T(4,128)(2,1)S(1)}, bf16[4096,4]{0,1:T(4,128)(2,1)}, u32[]{:S(2)}) copy-start(bf16[4096,4]{0,1:T(4,128)(2,1)} %param.26) | copy-start | bytes 98308
  136.5 7.9 %all-to-all-start.1 = ((s32[4,16,2]{1,2,0:T(2,128)}), s32[4,16,2]{1,2,0:T(2,128)S(1)}, u32[]{:S(2)}, u32[]{:S(2)}) async-start(s32[4,16,2]{1,2,0:T(2,128)} %fusion.48), calls=%async_computation.3 | async-start | bytes 8192 | tf_op jit(solution)/shard_map/all_to_all | solution.py:118
  166.2 8.6 %all-to-all-start.2 = ((bf16[4,16,512]{2,1,0:T(8,128)(2,1)}), bf16[4,16,512]{2,1,0:T(8,128)(2,1)S(1)}, u32[]{:S(2)}, u32[]{:S(2)}) async-start(bf16[4,16,512]{2,1,0:T(8,128)(2,1)} %bitcast.10), calls=%async_computation.4 | async-start | bytes 131072 | tf_op jit(solution)/shard_map/all_to_all | solution.py:158
Sparse Core Ops, SparseCore 0:
  53.0 28.9 reduce-scatter.2
  135.4 29.0 reduce-scatter.4
